TPU v7x, 32 devices: a whole 2x2x4 slice. The times are simulated.
32 devices in a mesh: sp: 8 (over z, y), tp: 4 (over x, core).
Axes of the slice: x: 2, y: 2, z: 4, core: 2. Of those that a mesh axis runs over, the one named last changes fastest.
Arguments:
- mixer_value_projection: bfloat16 [6144, 2048], P('sp', 'tp'), may hold values from -6 to 6
- write_vectors_projected: bfloat16 [6144, 256], P('sp', 'tp'), may hold values from -6 to 6
- read_vectors_projected: bfloat16 [6144, 256], P('sp', 'tp'), may hold values from -6 to 6
- output_gate_projected: bfloat16 [6144, 2048], P('sp', 'tp'), may hold values from -6 to 6
- step_size_scores: float32 [6144, 32], P('sp', 'tp'), may hold values from -8 to 8
- position_decay_extra: float32 [6144, 32], P('sp', 'tp'), may hold values from -1 to 0
- step_size_bias: float32 [32], P('tp'), may hold values from -1 to 1
- head_decay_logarithm: float32 [32], P('tp'), may hold values from -14 to -3
- value_filter_taps: bfloat16 [4, 2048], P(None, 'tp'), may hold values from -3 to 3
- write_filter_taps: bfloat16 [4, 256], P(None, 'tp'), may hold values from -3 to 3
- read_filter_taps: bfloat16 [4, 256], P(None, 'tp'), may hold values from -3 to 3
- gated_group_norm_gain: float32 [2048], P('tp'), may hold values from 0.1 to 1.9
- mixer_output_weight: bfloat16 [2048, 2048], P('tp'), may hold values from -0.125 to 0.125
- residual: bfloat16 [6144, 2048], P('sp'), may hold values from -6 to 6
- feedforward_norm_gain: float32 [2048], replicated, may hold values from 0.1 to 1.9
- feedforward_gate_weight: bfloat16 [2048, 5632], P('sp', 'tp'), may hold values from -0.125 to 0.125
- feedforward_value_weight: bfloat16 [2048, 5632], P('sp', 'tp'), may hold values from -0.125 to 0.125
- gate_filter_taps: bfloat16 [3, 5632], P(None, 'tp'), may hold values from -3.5 to 3.5
- single_value_filter_taps: bfloat16 [3, 5632], P(None, 'tp'), may hold values from -3.5 to 3.5
- feedforward_down_weight: bfloat16 [5632, 2048], P('tp', 'sp'), may hold values from -0.078125 to 0.078125
Outputs:
- mixed: bfloat16 [6144, 2048], P(('sp', 'tp'))
All inputs are finite; a program needn't handle non-finite values.
Results may differ from a plain program's by a relative error of at most 0.012.
Values may be sent and summed in bfloat16 or wider, within the bound.
A program may use at most 192 MiB of HBM per device.

v0:
```python
import jax
import jax.numpy as jnp
from jax import lax
from jax.sharding import PartitionSpec as P

HEAD = 64
STATE = 64
BLOCK = 128
epsilon = 1e-06


def from_behind(value, axis, by):
    length = lax.axis_size(axis)
    pairs = [(i, i + by) for i in range(length) if 0 <= i + by < length]
    return lax.ppermute(value, axis, pairs)


def entering_2(value, axis, join, neutral):
    count, mine = (lax.axis_size(axis), lax.axis_index(axis))
    pieces = jax.tree.map(lambda part: lax.all_gather(part, axis), value)
    running = jax.tree.map(
        lambda part, zero: jnp.full_like(part, 0) + jnp.asarray(zero, part.dtype), value, neutral
    )

    def lap(position, running):
        longer = join(running, jax.tree.map(lambda part: part[position], pieces))
        return jax.tree.map(lambda new, old: jnp.where(position < mine, new, old), longer, running)

    return lax.fori_loop(0, count - 1, lap, running)


def causal_taps(current, previous, kernel):
    tap_count = kernel.shape[0]
    length = current.shape[0]
    padded = jnp.concatenate([previous, current], 0).astype(jnp.float32)
    result = jnp.zeros((length, current.shape[1]), jnp.float32)
    for offset in range(tap_count):
        result = result + kernel[offset].astype(jnp.float32) * padded[offset : offset + length]
    return result


def channel_norm(stream, gain):
    floats = stream.astype(jnp.float32)
    scaled = floats * lax.rsqrt(jnp.mean(floats * floats, axis=-1, keepdims=True) + epsilon)
    return (scaled * gain).astype(jnp.bfloat16)


def on_device(
    mixer_value_projection,
    write_vectors_projected,
    read_vectors_projected,
    output_gate_projected,
    step_size_scores,
    position_decay_extra,
    step_size_bias,
    head_decay_logarithm,
    value_filter_taps,
    write_filter_taps,
    read_filter_taps,
    gated_group_norm_gain,
    mixer_output_weight,
    residual,
    feedforward_norm_gain,
    feedforward_gate_weight,
    feedforward_value_weight,
    gate_filter_taps,
    single_value_filter_taps,
    feedforward_down_weight,
):
    row_count = mixer_value_projection.shape[0]
    head_count = step_size_scores.shape[1]
    group_count = write_vectors_projected.shape[1] // STATE
    per_group = head_count // group_count
    mix_rim = value_filter_taps.shape[0] - 1
    rim_values, rim_write, rim_read = from_behind(
        (
            mixer_value_projection[row_count - mix_rim :],
            write_vectors_projected[row_count - mix_rim :],
            read_vectors_projected[row_count - mix_rim :],
        ),
        "sp",
        1,
    )
    x_conv = jax.nn.silu(causal_taps(mixer_value_projection, rim_values, value_filter_taps)).astype(
        jnp.bfloat16
    )
    write_conv = jax.nn.silu(
        causal_taps(write_vectors_projected, rim_write, write_filter_taps)
    ).astype(jnp.bfloat16)
    read_conv = jax.nn.silu(causal_taps(read_vectors_projected, rim_read, read_filter_taps)).astype(
        jnp.bfloat16
    )
    step_size_head = jax.nn.softplus(step_size_scores + step_size_bias)
    logarithm_decay_rate = -step_size_head * jnp.exp(head_decay_logarithm) + position_decay_extra
    scaled = (
        x_conv.astype(jnp.float32).reshape(row_count, head_count, HEAD) * step_size_head[:, :, None]
    ).astype(jnp.bfloat16)
    block_count = row_count // BLOCK
    value_blocks = scaled.reshape(block_count, BLOCK, group_count, per_group, HEAD)
    write_blocks = write_conv.reshape(block_count, BLOCK, group_count, STATE)
    read_blocks = read_conv.reshape(block_count, BLOCK, group_count, STATE)
    running = jnp.cumsum(logarithm_decay_rate.reshape(block_count, BLOCK, head_count), axis=1)
    by_head = jnp.moveaxis(running, 1, 2)
    spread = by_head[..., :, None] - by_head[..., None, :]
    causal = jnp.tril(jnp.ones((BLOCK, BLOCK), dtype=jnp.bool_))
    decays = jnp.exp(jnp.where(causal, spread, -jnp.inf)).reshape(
        block_count, group_count, per_group, BLOCK, BLOCK
    )
    scores = jnp.einsum(
        "blgn,bsgn->bgls", read_blocks, write_blocks, preferred_element_type=jnp.float32
    )
    weights = (scores[:, :, None] * decays).astype(jnp.bfloat16)
    inside = jnp.einsum(
        "bgrls,bsgrp->blgrp", weights, value_blocks, preferred_element_type=jnp.float32
    )
    tails = jnp.moveaxis(jnp.exp(by_head[..., -1:] - by_head), 2, 1).reshape(
        block_count, BLOCK, group_count, per_group
    )
    tailed = (value_blocks.astype(jnp.float32) * tails[..., None]).astype(jnp.bfloat16)
    fresh = jnp.einsum(
        "bsgn,bsgrp->bgrnp", write_blocks, tailed, preferred_element_type=jnp.float32
    )
    block_logs = by_head[..., -1].reshape(block_count, group_count, per_group)

    def carry_step(carried, inputs):
        piece, block_log = inputs
        return (carried * jnp.exp(block_log)[..., None, None] + piece, carried)

    empty_state = jnp.zeros((group_count, per_group, STATE, HEAD), jnp.float32)
    local_end, local_before = lax.scan(carry_step, empty_state, (fresh, block_logs))
    device_log = jnp.sum(block_logs, axis=0)

    def combine(earlier, later):
        return (earlier[0] * later[0], earlier[1] * later[0][..., None, None] + later[1])

    identity = (jnp.ones((group_count, per_group), jnp.float32), empty_state)
    incoming = entering_2((jnp.exp(device_log), local_end), "sp", combine, identity)[1]
    before_block = jnp.cumsum(block_logs, axis=0) - block_logs
    entering_state = local_before + incoming[None] * jnp.exp(before_block)[..., None, None]
    entering = jnp.einsum(
        "blgn,bgrnp->blgrp",
        read_blocks.astype(jnp.float32),
        entering_state,
        precision=lax.Precision.HIGHEST,
    )
    entering = (
        entering * jnp.exp(running).reshape(block_count, BLOCK, group_count, per_group)[..., None]
    )
    mixer = (inside + entering).reshape(row_count, head_count * HEAD)
    gated = (mixer * jax.nn.silu(output_gate_projected.astype(jnp.float32))).reshape(
        row_count, group_count, -1
    )
    gated = gated * lax.rsqrt(jnp.mean(gated * gated, axis=-1, keepdims=True) + epsilon)
    normed = (gated.reshape(row_count, -1) * gated_group_norm_gain).astype(jnp.bfloat16)
    share = row_count // lax.axis_size("tp")
    tp_index = lax.axis_index("tp")
    summed = lax.psum_scatter(
        jnp.dot(normed, mixer_output_weight, preferred_element_type=jnp.float32),
        "tp",
        scatter_dimension=0,
        tiled=True,
    )
    own_residual = lax.dynamic_slice_in_dim(residual, tp_index * share, share, 0)
    stream = (own_residual.astype(jnp.float32) + summed).astype(jnp.bfloat16)
    ffn_rows = lax.all_gather(channel_norm(stream, feedforward_norm_gain), "tp", axis=0, tiled=True)
    gate_full, value_full = (
        lax.all_gather(feedforward_gate_weight, "sp", axis=0, tiled=True),
        lax.all_gather(feedforward_value_weight, "sp", axis=0, tiled=True),
    )
    gate_sum = jnp.dot(ffn_rows, gate_full, preferred_element_type=jnp.float32)
    value_sum = jnp.dot(ffn_rows, value_full, preferred_element_type=jnp.float32)
    gate_rows = gate_sum.astype(jnp.bfloat16)
    value_rows = value_sum.astype(jnp.bfloat16)
    ffn_rim = gate_filter_taps.shape[0] - 1
    rim_gate, rim_value = from_behind(
        (gate_rows[row_count - ffn_rim :], value_rows[row_count - ffn_rim :]), "sp", 1
    )
    hidden = (
        jax.nn.silu(causal_taps(gate_rows, rim_gate, gate_filter_taps))
        * causal_taps(value_rows, rim_value, single_value_filter_taps)
    ).astype(jnp.bfloat16)
    down_full = lax.all_gather(feedforward_down_weight, "sp", axis=1, tiled=True)
    partial_down = jnp.dot(hidden, down_full, preferred_element_type=jnp.float32)
    down = lax.psum_scatter(
        partial_down.astype(jnp.bfloat16), "tp", scatter_dimension=0, tiled=True
    ).astype(jnp.float32)
    return (stream.astype(jnp.float32) + down).astype(jnp.bfloat16)


def solution(mesh):
    placed = (
        P("sp", "tp"),
        P("sp", "tp"),
        P("sp", "tp"),
        P("sp", "tp"),
        P("sp", "tp"),
        P("sp", "tp"),
        P("tp"),
        P("tp"),
        P(None, "tp"),
        P(None, "tp"),
        P(None, "tp"),
        P("tp"),
        P("tp", None),
        P("sp", None),
        P(),
        P("sp", "tp"),
        P("sp", "tp"),
        P(None, "tp"),
        P(None, "tp"),
        P("tp", "sp"),
    )
    return jax.shard_map(
        on_device, mesh=mesh, in_specs=placed, out_specs=P(("sp", "tp"), None), check_vma=False
    )
```

profile of v0, /device:TPU:0, one launch (start us, length us, event | category | flops | bytes accessed | tf_op | source)
XLA Modules:
  0.0 557.1 jit_solution(11165353216714825185)
XLA Ops:
  8.2 5.7 %collective-permute-start = (bf16[3,512]{0,1:T(8,128)(2,1)}, bf16[3,512]{0,1:T(8,128)(2,1)}, u32[]{:S(2)}, u32[]{:S(2)}) collective-permute-start(bf16[3,512]{0,1:T(8,128)(2,1)} %copy.49), channel_id=1, source_target_pairs={{0,4},{4,8},{8,12},{12,16},{16,20},{20,24},{24,28},{1,5},{5,9},{9,... | collective-permute-start | bytes 9224 | tf_op jit(solution)/shard_map/ppermute | solution.py:15
  13.9 1.4 slice.146
  15.3 3.5 collective-permute-start.2
  18.8 2.3 copy.50
  21.1 1.4 slice_convert_fusion.3
  23.1 1.5 fusion.53
  25.2 1.1 slice_reduce_fusion
  30.6 1.6 maximum_convert_fusion.2
  32.2 2.7 fusion.39
  34.9 2.7 reshape.164
  37.6 2.9 multiply_convert_fusion.1
  40.5 1.5 convolution_bitcast_fusion
  42.0 15.6 %while.27 = (s32[]{:T(128)}, f32[1,8,64,64]{3,2,1,0:T(8,128)S(1)}, f32[6,1,8,64,64]{4,3,2,1,0:T(8,128)}, f32[6,1,8]{2,1,0:T(1,128)}, f32[6,1,8,64,64]{3,4,2,0,1:T(8,128)}, /*index=5*/s32[]{:T(128)}, s32[]{:T(128)}) while((s32[]{:T(128)}, f32[1,8,64,64]{3,2,1,0:T(8,128)S(1)}, f32[6,1,8,64,64]{4,3,2,1,0:T(8,128)}, ...), condition=%wide.region_2.3_spmd.clone, body=%wide.region_1.2_spmd.clone.sunk | while | flops 131075 | bytes 1311424 | solution.py:130
  59.2 2.8 collective-permute-start.1
  62.2 1.2 dynamic-slice
  64.8 19.2 %all-reduce = f32[64]{0:T(128)S(1)} all-reduce(f32[64]{0:T(128)S(1)} %exponential_dynamic-update-slice_fusion), channel_id=2, replica_groups=mesh['sp'=8,'tp'=4] {'sp'}, use_global_device_ids=true, to_apply=%add | all-reduce | flops 64 | bytes 512
  84.2 1.1 copy.66
  85.3 2.3 copy.68
  88.2 1.6 fusion.46
  89.7 17.8 %all-gather.16.cloned.1.call-done = f32[8,8,64,64]{3,2,1,0:T(8,128)} async-done(((f32[1,8,64,64]{3,2,1,0:T(8,128)}), f32[8,8,64,64]{3,2,1,0:T(8,128)}) %all-gather.16.cloned.1.call-update) | async-done | bytes 1048592 | tf_op jit(solution)/shard_map/all_gather | solution.py:20
  107.5 7.6 %while.28 = (s32[]{:T(128)}, f32[1,8,64,64]{3,2,1,0:T(8,128)S(1)}, s32[]{:T(128)}, f32[8,1,8]{2,1,0:T(1,128)S(1)}, f32[8,1,8,64,64]{4,3,2,1,0:T(8,128)}, /*index=5*/s32[]{:T(128)}, s32[]{:T(128)}) while((s32[]{:T(128)}, f32[1,8,64,64]{3,2,1,0:T(8,128)S(1)}, s32[]{:T(128)}, f32[8,1,8]{2,1,0:T(1,128)S(1)}, ...), condition=%wide.region_5.6_spmd.clone, body=%wide.region_4.5_spmd.clone.sunk | while | flops 131076 | bytes 393417 | solution.py:29
  107.5 1.0 fusion.73
  108.6 1.1 fusion.73
  109.7 1.1 fusion.73
  110.8 1.1 fusion.73
  111.8 1.1 fusion.73
  112.9 1.1 fusion.73
  114.0 1.1 fusion.73
  115.1 3.0 fusion.23
  118.1 1.3 fusion.22
  121.1 4.8 fusion.32
  126.7 56.8 %reduce-scatter.3.cloned.1.call-done = f32[192,2048]{1,0:T(8,128)} async-done(((f32[768,2048]{1,0:T(8,128)}), f32[192,2048]{1,0:T(8,128)}) %reduce-scatter.3.cloned.1.call-update) | async-done | bytes 1572880 | tf_op jit(solution)/shard_map/reduce_scatter | solution.py:157
  183.5 1.9 fusion.14
  185.5 1.1 fusion.16
  188.0 90.1 %all-gather.10.cloned.1.call-done = bf16[2048,1408]{1,0:T(8,128)(2,1)} async-done(((bf16[256,1408]{1,0:T(8,128)(2,1)}), bf16[2048,1408]{1,0:T(8,128)(2,1)}) %all-gather.10.cloned.1.call-update) | async-done | bytes 5767184 | tf_op jit(solution)/shard_map/all_gather | solution.py:167
  278.0 28.1 %all-gather.8.cloned.1.call-done = bf16[768,2048]{1,0:T(8,128)(2,1)} async-done(((bf16[192,2048]{1,0:T(8,128)(2,1)}), bf16[768,2048]{1,0:T(8,128)(2,1)}) %all-gather.8.cloned.1.call-update) | async-done | bytes 3145744 | tf_op jit(solution)/shard_map/all_gather | solution.py:165
  306.2 8.3 %convolution_convert_fusion.2 = bf16[768,1408]{1,0:T(8,128)(2,1)S(1)} fusion(bf16[768,2048]{1,0:T(8,128)(2,1)} %all-gather.8.cloned.1.call-done, bf16[2048,1408]{1,0:T(8,128)(2,1)} %all-gather.10.cloned.1.call-done), kind=kOutput, calls=%fused_computation.23 | convolution fusion | flops 4430266368 | bytes 11075584 | tf_op jit(solution)/shard_map/dot_general | solution.py:170
  314.5 1.3 copy-done.4
  315.9 3.4 collective-permute-start.3
  319.3 81.4 %all-gather.12.cloned.1.call-done = bf16[2048,1408]{1,0:T(8,128)(2,1)} async-done(((bf16[256,1408]{1,0:T(8,128)(2,1)}), bf16[2048,1408]{1,0:T(8,128)(2,1)}) %all-gather.12.cloned.1.call-update) | async-done | bytes 5767184 | tf_op jit(solution)/shard_map/all_gather | solution.py:168
  400.7 8.5 %convolution_convert_fusion.1 = bf16[768,1408]{1,0:T(8,128)(2,1)S(1)} fusion(bf16[768,2048]{1,0:T(8,128)(2,1)} %all-gather.8.cloned.1.call-done, bf16[2048,1408]{1,0:T(8,128)(2,1)} %all-gather.12.cloned.1.call-done), kind=kOutput, calls=%fused_computation.22 | convolution fusion | flops 4430266368 | bytes 11075584 | tf_op jit(solution)/shard_map/dot_general | solution.py:171
  409.2 2.7 collective-permute-start.4
  411.9 2.4 maximum_convert_fusion
  414.3 2.5 maximum_convert_fusion.1
  416.9 77.2 %all-gather.14.cloned.1.call-done = bf16[1408,2048]{1,0:T(8,128)(2,1)} async-done(((bf16[1408,256]{1,0:T(8,128)(2,1)}), bf16[1408,2048]{1,0:T(8,128)(2,1)}) %all-gather.14.cloned.1.call-update) | async-done | bytes 5767184 | tf_op jit(solution)/shard_map/all_gather | solution.py:182
  494.1 17.6 %convolution_convert_fusion = bf16[768,2048]{1,0:T(8,128)(2,1)} fusion(bf16[1408,2048]{1,0:T(8,128)(2,1)} %all-gather.14.cloned.1.call-done, f32[770,1408]{1,0:T(8,128)} %maximum_convert_fusion.1, f32[770,1408]{1,0:T(8,128)} %maximum_convert_fusion, f32[1408]{0:T(1024)S(1)} %get-tuple-element.200, f32[1408]{0:T(1024)S(1)} %get-tuple-element.201, ...), kind=kOutput, calls=%fused_computation.21 | convolution fusion | flops 4448059392 | bytes 34898944 | tf_op jit(solution)/shard_map/dot_general | solution.py:183
  511.8 36.2 %reduce-scatter.5.cloned.1.call-done = bf16[192,2048]{1,0:T(8,128)(2,1)} async-done(((bf16[768,2048]{1,0:T(8,128)(2,1)}), bf16[192,2048]{1,0:T(8,128)(2,1)}) %reduce-scatter.5.cloned.1.call-update) | async-done | bytes 786448 | tf_op jit(solution)/shard_map/reduce_scatter | solution.py:184
  548.0 2.3 fusion.17
  (134 shorter events, 29.4 us)
Async XLA Ops:
  6.5 114.6 %copy-start = (bf16[512,2048]{1,0:T(8,128)(2,1)S(1)}, bf16[512,2048]{1,0:T(8,128)(2,1)}, u32[]{:S(2)}) copy-start(bf16[512,2048]{1,0:T(8,128)(2,1)} %param.36) | copy-start | bytes 6291460
  6.5 100.9 %all-gather.16.cloned.1.call-start = ((), (), s32[]{:S(2)}) async-start(), calls=%async_computation.8 | async-start | bytes 2359296 | tf_op jit(solution)/shard_map/all_gather | solution.py:20
  8.2 19.0 %copy-start.14 = (bf16[4,64]{1,0:T(4,128)(2,1)S(1)}, bf16[4,64]{1,0:T(4,128)(2,1)}, u32[]{:S(2)}) copy-start(bf16[4,64]{1,0:T(4,128)(2,1)} %param.33) | copy-start | bytes 1540
  8.2 22.4 %collective-permute-start = (bf16[3,512]{0,1:T(8,128)(2,1)}, bf16[3,512]{0,1:T(8,128)(2,1)}, u32[]{:S(2)}, u32[]{:S(2)}) collective-permute-start(bf16[3,512]{0,1:T(8,128)(2,1)} %copy.49), channel_id=1, source_target_pairs={{0,4},{4,8},{8,12},{12,16},{16,20},{20,24},{24,28},{1,5},{5,9},{9,... | collective-permute-start | bytes 9224 | tf_op jit(solution)/shard_map/ppermute | solution.py:15
  15.3 13.5 %copy-start.7 = (bf16[768,64]{0,1:T(8,128)(2,1)S(1)}, bf16[768,64]{0,1:T(8,128)(2,1)}, u32[]{:S(2)}) copy-start(bf16[768,64]{0,1:T(8,128)(2,1)} %param.25) | copy-start | bytes 294916
  15.3 13.4 %collective-permute-start.2 = (bf16[3,64]{0,1:T(8,128)(2,1)}, bf16[3,64]{0,1:T(8,128)(2,1)}, u32[]{:S(2)}, u32[]{:S(2)}) collective-permute-start(bf16[3,64]{0,1:T(8,128)(2,1)} %slice.146), channel_id=1, source_target_pairs={{0,4},{4,8},{8,12},{12,16},{16,20},{20,24},{24,28},{1,5},{5,9},{9,... | collective-permute-start | bytes 1160 | tf_op jit(solution)/shard_map/ppermute | solution.py:15
  28.7 3.5 copy-start.12
  28.7 3.5 copy-start.13
  42.0 42.1 %copy-start.15 = (bf16[4,64]{1,0:T(4,128)(2,1)S(1)}, bf16[4,64]{1,0:T(4,128)(2,1)}, u32[]{:S(2)}) copy-start(bf16[4,64]{1,0:T(4,128)(2,1)} %param.34) | copy-start | bytes 1540
  57.6 0.7 copy-start.2
  57.6 30.0 %copy-start.8 = (bf16[768,64]{0,1:T(8,128)(2,1)S(1)}, bf16[768,64]{0,1:T(8,128)(2,1)}, u32[]{:S(2)}) copy-start(bf16[768,64]{0,1:T(8,128)(2,1)} %param.26) | copy-start | bytes 294916
  57.6 30.5 %copy-start.16 = (f32[64]{0:T(128)S(1)}, f32[64]{0:T(128)}, u32[]{:S(2)}) copy-start(f32[64]{0:T(128)} %get-tuple-element.241) | copy-start | bytes 772
  57.6 30.5 %copy-start.17 = (f32[64]{0:T(128)S(1)}, f32[64]{0:T(128)}, u32[]{:S(2)}) copy-start(f32[64]{0:T(128)} %get-tuple-element.242) | copy-start | bytes 772
  57.7 30.5 %copy-start.18 = (f32[64]{0:T(128)S(1)}, f32[64]{0:T(128)}, u32[]{:S(2)}) copy-start(f32[64]{0:T(128)} %get-tuple-element.243) | copy-start | bytes 772
  57.7 30.5 %copy-start.19 = (f32[64]{0:T(128)S(1)}, f32[64]{0:T(128)}, u32[]{:S(2)}) copy-start(f32[64]{0:T(128)} %get-tuple-element.244) | copy-start | bytes 772
  58.4 125.2 %reduce-scatter.3.cloned.1.call-start = ((), (), s32[]{:S(2)}) async-start(), calls=%async_computation.2 | async-start | bytes 7864320 | tf_op jit(solution)/shard_map/reduce_scatter | solution.py:157
  59.2 28.4 %collective-permute-start.1 = (bf16[3,64]{0,1:T(8,128)(2,1)S(1)}, bf16[3,64]{0,1:T(8,128)(2,1)S(1)}, u32[]{:S(2)}, u32[]{:S(2)}) collective-permute-start(bf16[3,64]{0,1:T(8,128)(2,1)S(1)} %slice.137), channel_id=1, source_target_pairs={{0,4},{4,8},{8,12},{12,16},{16,20},{20,24},{24,28},{1,5},{5,9},{9,... | collective-permute-start | bytes 1160 | tf_op jit(solution)/shard_map/ppermute | solution.py:15
  115.1 3.0 copy-start.6
  115.1 3.0 copy-start.21
  119.4 1.1 copy-start.3
  120.3 0.8 copy-start.20
  125.9 59.5 %copy-start.11 = (f32[2048]{0:T(1024)S(1)}, f32[2048]{0:T(1024)}, u32[]{:S(2)}) copy-start(f32[2048]{0:T(1024)} %param.38) | copy-start | bytes 24580
  126.0 152.1 %all-gather.10.cloned.1.call-start = ((), (), s32[]{:S(2)}) async-start(), calls=%async_computation.4 | async-start | bytes 6488064 | tf_op jit(solution)/shard_map/all_gather | solution.py:167
  126.7 179.5 %all-gather.8.cloned.1.call-start = ((), (), s32[]{:S(2)}) async-start(), calls=%async_computation.3 | async-start | bytes 3932160 | tf_op jit(solution)/shard_map/all_gather | solution.py:165
  185.4 2.4 copy-start.9
  185.4 2.4 copy-start.10
  186.6 214.1 %all-gather.12.cloned.1.call-start = ((), (), s32[]{:S(2)}) async-start(), calls=%async_computation.5 | async-start | bytes 6488064 | tf_op jit(solution)/shard_map/all_gather | solution.py:168
  187.2 306.9 %all-gather.14.cloned.1.call-start = ((), (), s32[]{:S(2)}) async-start(), calls=%async_computation.6 | async-start | bytes 6488064 | tf_op jit(solution)/shard_map/all_gather | solution.py:182
  187.8 360.2 %reduce-scatter.5.cloned.1.call-start = ((), (), s32[]{:S(2)}) async-start(), calls=%async_computation.7 | async-start | bytes 3932160 | tf_op jit(solution)/shard_map/reduce_scatter | solution.py:184
  314.5 1.3 copy-start.4
  315.9 96.0 %collective-permute-start.3 = (bf16[2,1408]{1,0:T(2,128)(2,1)S(1)}, bf16[2,1408]{1,0:T(2,128)(2,1)S(1)}, u32[]{:S(2)}, u32[]{:S(2)}) collective-permute-start(bf16[2,1408]{1,0:T(2,128)(2,1)S(1)} %slice.182), channel_id=1, source_target_pairs={{0,4},{4,8},{8,12},{12,16},{16,20},{20,24},{24,28},{1,5},{5,9},{9,... | collective-permute-start | bytes 16904 | tf_op jit(solution)/shard_map/ppermute | solution.py:15
  400.7 11.2 %copy-start.5 = (bf16[768,1408]{1,0:T(8,128)(2,1)S(1)}, bf16[768,1408]{1,0:T(8,128)(2,1)}, u32[]{:S(2)}) copy-start(bf16[768,1408]{1,0:T(8,128)(2,1)} %copy-done.4) | copy-start | bytes 6488068
  409.2 5.1 collective-permute-start.4
  511.8 38.5 %copy-start.1 = (bf16[512,2048]{1,0:T(8,128)(2,1)S(1)}, bf16[512,2048]{1,0:T(8,128)(2,1)}, u32[]{:S(2)}) copy-start(bf16[512,2048]{1,0:T(8,128)(2,1)} %param.36) | copy-start | bytes 6291460
Sparse Core Ops, SparseCore 0:
  58.5 48.9 all-gather.15
  126.1 57.4 reduce-scatter.2
  185.7 92.2 all-gather.9
  279.5 26.6 all-gather.7
  308.2 92.4 all-gather.11
  402.6 91.5 all-gather.13
  511.9 36.0 reduce-scatter.4
where the time goes:
time: 559 us; the launch traced here: 557 us
  waiting for transfers between devices  389 us (70%)
  matrix products  46.6 us (8%)
  other arithmetic  38.4 us (7%)
  local copies, waits for them, and re-layouts  30.2 us (5%)
  blocking collectives  19.2 us (3%)
  starting transfers between devices  18.3 us (3%)
  between operations  14.6 us (3%)
    all_gather x1, waiting for transfers between devices, on_device(): lax.all_gather(feedforward_gate_weight, 'sp', axis=0, tiled=True)  90.1 us
    all_gather x1, waiting for transfers between devices, on_device(): lax.all_gather(feedforward_value_weight, 'sp', axis=0, tiled=True)  81.4 us
    all_gather x1, waiting for transfers between devices, on_device(): lax.all_gather(feedforward_down_weight, 'sp', axis=1, tiled=True)  77.2 us
    reduce_scatter x1, waiting for transfers between devices, on_device(): lax.psum_scatter(jnp.dot(normed, mixer_output_weight, preferred_element_t...  56.8 us
    reduce_scatter x1, waiting for transfers between devices, on_device(): lax.psum_scatter(partial_down.astype(jnp.bfloat16), 'tp', scatter_dimensi...  36.2 us
    all_gather x1, waiting for transfers between devices, on_device(): lax.all_gather(channel_norm(stream, feedforward_norm_gain), 'tp', axis=0,...  28.1 us
    unnamed x1, blocking collectives  19.2 us
    ppermute x5, starting transfers between devices, from_behind(): return lax.ppermute(value, axis, pairs)  18.1 us
  transfers between devices with their start and end apart: 12, of which 7 were waited for; matrix products, arithmetic and copies ran while one was open for 8% of the time, Pallas kernels for 0%

commit v1 on v0

--- a/solution.py
+++ b/solution.py
@@ -179,7 +179,12 @@
         jax.nn.silu(causal_taps(gate_rows, rim_gate, gate_filter_taps))
         * causal_taps(value_rows, rim_value, single_value_filter_taps)
     ).astype(jnp.bfloat16)
-    down_full = lax.all_gather(feedforward_down_weight, "sp", axis=1, tiled=True)
+    ring = [feedforward_down_weight]
+    for hop in range(7):
+        ring.append(lax.ppermute(ring[-1], "sp", [(dev, (dev + 1) % 8) for dev in range(8)]))
+    down_full = jnp.roll(
+        jnp.concatenate(ring[::-1], axis=1), (lax.axis_index("sp") + 1) * ring[0].shape[1], axis=1
+    )
     partial_down = jnp.dot(hidden, down_full, preferred_element_type=jnp.float32)
     down = lax.psum_scatter(
         partial_down.astype(jnp.bfloat16), "tp", scatter_dimension=0, tiled=True

time: 559 us -> 540 us (0.966)
  waiting for transfers between devices: 389 us -> 351 us
  local copies, waits for them, and re-layouts: 30.2 us -> 53.1 us
    ppermute x0 -> x7, waiting for transfers between devices: none -> 199 us  [on_device(): lax.ppermute(ring[-1], 'sp', [(dev, (dev + 1) % 8) for dev in range(8)])]
    all_gather x1, waiting for transfers between devices: 81.4 us -> 0.01 us  [on_device(): lax.all_gather(feedforward_value_weight, 'sp', axis=0, tiled=True)]
    all_gather x1 -> x0, waiting for transfers between devices: 77.2 us -> none  [on_device(): lax.all_gather(feedforward_down_weight, 'sp', axis=1, tiled=True)]
    all_gather x1, waiting for transfers between devices: 90.1 us -> 38.1 us  [on_device(): lax.all_gather(feedforward_gate_weight, 'sp', axis=0, tiled=True)]
    all_gather x1, waiting for transfers between devices: 28.1 us -> 0.01 us  [on_device(): lax.all_gather(channel_norm(stream, feedforward_norm_gain), 'tp', axis=0,...]
    unnamed x50 -> x75, local copies, waits for them, and re-layouts: 8.84 us -> 31.1 us
  transfers between devices with their start and end apart: 12 -> 18, of which waited for: 7 -> 12; matrix products, arithmetic and copies ran while one was open for 8% -> 12% of each run, Pallas kernels for 0% -> 0%
where the time goes in v1:
time: 540 us; the launch traced here: 538 us
  waiting for transfers between devices  351 us (65%)
  local copies, waits for them, and re-layouts  53.1 us (10%)
  matrix products  43.8 us (8%)
  other arithmetic  38.6 us (7%)
  blocking collectives  19.2 us (4%)
  starting transfers between devices  17.5 us (3%)
  between operations  14.7 us (3%)
    ppermute x7, waiting for transfers between devices, on_device(): lax.ppermute(ring[-1], 'sp', [(dev, (dev + 1) % 8) for dev in range(8)])  199 us
    reduce_scatter x1, waiting for transfers between devices, on_device(): lax.psum_scatter(jnp.dot(normed, mixer_output_weight, preferred_element_t...  56.7 us
    reduce_scatter x1, waiting for transfers between devices, on_device(): lax.psum_scatter(partial_down.astype(jnp.bfloat16), 'tp', scatter_dimensi...  38.8 us
    all_gather x1, waiting for transfers between devices, on_device(): lax.all_gather(feedforward_gate_weight, 'sp', axis=0, tiled=True)  38.1 us
    unnamed x75, local copies, waits for them, and re-layouts  31.1 us
    unnamed x1, blocking collectives  19.2 us
    all_gather x1, waiting for transfers between devices, entering_2(): pieces = jax.tree.map(lambda part: lax.all_gather(part, axis), value)  16.8 us
    ppermute x5, starting transfers between devices, from_behind(): return lax.ppermute(value, axis, pairs)  15.8 us
  transfers between devices with their start and end apart: 18, of which 12 were waited for; matrix products, arithmetic and copies ran while one was open for 12% of the time, Pallas kernels for 0%

profile of v1, /device:TPU:0, one launch (start us, length us, event | category | flops | bytes accessed | tf_op | source)
XLA Modules:
  0.0 538.0 jit_solution(17772516242664140963)
XLA Ops:
  7.6 4.9 collective-permute-start
  13.3 3.4 collective-permute-start.2
  19.2 1.4 reduce_window_sum.22
  20.6 1.1 slice_reduce_fusion
  22.7 1.4 slice_convert_fusion.3
  24.1 1.4 bitcast_convert_fusion.3
  25.6 2.3 copy.50
  27.8 1.2 copy.58
  30.3 1.6 maximum_convert_fusion.2
  31.8 3.4 fusion.44
  35.2 2.6 reshape.164
  37.9 2.9 multiply_convert_fusion.1
  40.8 1.5 convolution_bitcast_fusion
  42.3 15.6 %while.27 = (s32[]{:T(128)}, f32[1,8,64,64]{3,2,1,0:T(8,128)S(1)}, f32[6,1,8,64,64]{4,3,2,1,0:T(8,128)}, f32[6,1,8]{2,1,0:T(1,128)}, f32[6,1,8,64,64]{3,4,2,0,1:T(8,128)}, /*index=5*/s32[]{:T(128)}, s32[]{:T(128)}) while((s32[]{:T(128)}, f32[1,8,64,64]{3,2,1,0:T(8,128)S(1)}, f32[6,1,8,64,64]{4,3,2,1,0:T(8,128)}, ...), condition=%wide.region_2.3_spmd.clone, body=%wide.region_1.2_spmd.clone.sunk | while | flops 131075 | bytes 1310924 | solution.py:130
  59.5 3.4 collective-permute-start.1
  63.1 2.3 copy.68
  67.5 19.2 %all-reduce = f32[64]{0:T(128)S(1)} all-reduce(f32[64]{0:T(128)S(1)} %exponential_dynamic-update-slice_fusion), channel_id=2, replica_groups=mesh['sp'=8,'tp'=4] {'sp'}, use_global_device_ids=true, to_apply=%add | all-reduce | flops 64 | bytes 512
  89.4 2.1 fusion.51
  91.5 16.8 %all-gather.13.cloned.1.call-done = f32[8,8,64,64]{3,2,1,0:T(8,128)} async-done(((f32[1,8,64,64]{3,2,1,0:T(8,128)}), f32[8,8,64,64]{3,2,1,0:T(8,128)}) %all-gather.13.cloned.1.call-update) | async-done | bytes 1048592 | tf_op jit(solution)/shard_map/all_gather | solution.py:20
  108.3 7.7 %while.28 = (s32[]{:T(128)}, f32[1,8,64,64]{3,2,1,0:T(8,128)S(1)}, s32[]{:T(128)}, f32[8,1,8]{2,1,0:T(1,128)S(1)}, f32[8,1,8,64,64]{4,3,2,1,0:T(8,128)}, /*index=5*/s32[]{:T(128)}, s32[]{:T(128)}) while((s32[]{:T(128)}, f32[1,8,64,64]{3,2,1,0:T(8,128)S(1)}, s32[]{:T(128)}, f32[8,1,8]{2,1,0:T(1,128)S(1)}, ...), condition=%wide.region_5.6_spmd.clone, body=%wide.region_4.5_spmd.clone.sunk | while | flops 131076 | bytes 393425 | solution.py:29
  116.0 3.0 fusion.28
  119.0 1.3 fusion.27
  122.0 4.8 fusion.37
  127.6 56.7 %reduce-scatter.3.cloned.1.call-done = f32[192,2048]{1,0:T(8,128)} async-done(((f32[768,2048]{1,0:T(8,128)}), f32[192,2048]{1,0:T(8,128)}) %reduce-scatter.3.cloned.1.call-update) | async-done | bytes 1572880 | tf_op jit(solution)/shard_map/reduce_scatter | solution.py:157
  184.4 1.9 fusion.19
  186.3 1.1 fusion.21
  187.5 1.5 collective-permute-start.5
  189.1 27.6 %collective-permute-done.5 = bf16[1408,256]{1,0:T(8,128)(2,1)S(1)} collective-permute-done((bf16[1408,256]{1,0:T(8,128)(2,1)S(1)}, bf16[1408,256]{1,0:T(8,128)(2,1)S(1)}, u32[]{:S(2)}, u32[]{:S(2)}) %collective-permute-start.5) | collective-permute-done | bytes 720928 | tf_op jit(solution)/shard_map/ppermute | solution.py:184
  216.7 30.0 %collective-permute-done.6 = bf16[1408,256]{1,0:T(8,128)(2,1)S(1)} collective-permute-done((bf16[1408,256]{1,0:T(8,128)(2,1)S(1)}, bf16[1408,256]{1,0:T(8,128)(2,1)S(1)}, u32[]{:S(2)}, u32[]{:S(2)}) %collective-permute-start.6) | collective-permute-done | bytes 720928 | tf_op jit(solution)/shard_map/ppermute | solution.py:184
  247.6 36.3 %collective-permute-done.7 = bf16[1408,256]{1,0:T(8,128)(2,1)S(1)} collective-permute-done((bf16[1408,256]{1,0:T(8,128)(2,1)S(1)}, bf16[1408,256]{1,0:T(8,128)(2,1)S(1)}, u32[]{:S(2)}, u32[]{:S(2)}) %collective-permute-start.7) | collective-permute-done | bytes 720928 | tf_op jit(solution)/shard_map/ppermute | solution.py:184
  284.8 36.1 %collective-permute-done.8 = bf16[1408,256]{1,0:T(8,128)(2,1)S(1)} collective-permute-done((bf16[1408,256]{1,0:T(8,128)(2,1)S(1)}, bf16[1408,256]{1,0:T(8,128)(2,1)S(1)}, u32[]{:S(2)}, u32[]{:S(2)}) %collective-permute-start.8) | collective-permute-done | bytes 720928 | tf_op jit(solution)/shard_map/ppermute | solution.py:184
  321.8 21.2 %collective-permute-done.9 = bf16[1408,256]{1,0:T(8,128)(2,1)S(1)} collective-permute-done((bf16[1408,256]{1,0:T(8,128)(2,1)S(1)}, bf16[1408,256]{1,0:T(8,128)(2,1)S(1)}, u32[]{:S(2)}, u32[]{:S(2)}) %collective-permute-start.9) | collective-permute-done | bytes 720928 | tf_op jit(solution)/shard_map/ppermute | solution.py:184
  343.9 19.7 %collective-permute-done.10 = bf16[1408,256]{1,0:T(8,128)(2,1)} collective-permute-done((bf16[1408,256]{1,0:T(8,128)(2,1)S(1)}, bf16[1408,256]{1,0:T(8,128)(2,1)}, u32[]{:S(2)}, u32[]{:S(2)}) %collective-permute-start.10) | collective-permute-done | bytes 720928 | tf_op jit(solution)/shard_map/ppermute | solution.py:184
  363.7 27.7 %collective-permute-done.11 = bf16[1408,256]{1,0:T(8,128)(2,1)} collective-permute-done((bf16[1408,256]{1,0:T(8,128)(2,1)}, bf16[1408,256]{1,0:T(8,128)(2,1)}, u32[]{:S(2)}, u32[]{:S(2)}) %collective-permute-start.11) | collective-permute-done | bytes 720928 | tf_op jit(solution)/shard_map/ppermute | solution.py:184
  391.4 2.1 constant_dynamic-update-slice_fusion.15
  393.5 2.2 constant_dynamic-update-slice_fusion.14
  401.6 2.1 constant_dynamic-update-slice_fusion.7
  403.7 2.1 constant_dynamic-update-slice_fusion.6
  411.6 8.3 %convolution_convert_fusion = bf16[768,1408]{1,0:T(8,128)(2,1)S(1)} fusion(bf16[768,2048]{1,0:T(8,128)(2,1)} %all-gather.7.cloned.1.call-done, bf16[2048,1408]{1,0:T(8,128)(2,1)} %all-gather.11.cloned.1.call-done), kind=kOutput, calls=%fused_computation.24 | convolution fusion | flops 4430266368 | bytes 11075584 | tf_op jit(solution)/shard_map/dot_general | solution.py:171
  419.9 1.4 copy-done.13
  421.4 1.5 collective-permute-start.4
  422.9 38.1 %all-gather.9.cloned.1.call-done = bf16[2048,1408]{1,0:T(8,128)(2,1)} async-done(((bf16[256,1408]{1,0:T(8,128)(2,1)}), bf16[2048,1408]{1,0:T(8,128)(2,1)}) %all-gather.9.cloned.1.call-update) | async-done | bytes 5767184 | tf_op jit(solution)/shard_map/all_gather | solution.py:167
  461.0 8.5 %convolution_convert_fusion.1 = bf16[768,1408]{1,0:T(8,128)(2,1)S(1)} fusion(bf16[768,2048]{1,0:T(8,128)(2,1)} %all-gather.7.cloned.1.call-done, bf16[2048,1408]{1,0:T(8,128)(2,1)} %all-gather.9.cloned.1.call-done), kind=kOutput, calls=%fused_computation.25 | convolution fusion | flops 4430266368 | bytes 11075584 | tf_op jit(solution)/shard_map/dot_general | solution.py:170
  469.5 2.5 collective-permute-start.3
  473.4 2.4 maximum_convert_fusion
  475.8 14.3 %fusion.11 = bf16[768,2048]{1,0:T(8,128)(2,1)} fusion(bf16[1408,4096]{1,0:T(8,128)(2,1)} %constant_dynamic-update-slice_fusion, s32[]{:T(128)S(6)} %select_n.54, f32[770,1408]{1,0:T(8,128)S(1)} %maximum_convert_fusion.1, f32[770,1408]{1,0:T(8,128)} %maximum_convert_fusion, f32[1408]{0:T(1024)S(1)} %get-tuple-element.200, f32[1408]{0:T(1024)S(1)} %get-tuple-element.201, ...), kind=kOutput, calls=%fused_computation.23 | convolution fusion | flops 4448059392 | bytes 34914308 | tf_op jit(solution)/shard_map/dot_general | solution.py:188
  490.1 38.8 %reduce-scatter.5.cloned.1.call-done = bf16[192,2048]{1,0:T(8,128)(2,1)} async-done(((bf16[768,2048]{1,0:T(8,128)(2,1)}), bf16[192,2048]{1,0:T(8,128)(2,1)}) %reduce-scatter.5.cloned.1.call-update) | async-done | bytes 786448 | tf_op jit(solution)/shard_map/reduce_scatter | solution.py:189
  528.9 2.3 fusion.22
  (171 shorter events, 54.4 us)
Async XLA Ops:
  6.5 115.4 %copy-start = (bf16[512,2048]{1,0:T(8,128)(2,1)S(1)}, bf16[512,2048]{1,0:T(8,128)(2,1)}, u32[]{:S(2)}) copy-start(bf16[512,2048]{1,0:T(8,128)(2,1)} %param.36) | copy-start | bytes 6291460
  6.5 22.5 %copy-start.16 = (bf16[768,64]{0,1:T(8,128)(2,1)S(1)}, bf16[768,64]{0,1:T(8,128)(2,1)}, u32[]{:S(2)}) copy-start(bf16[768,64]{0,1:T(8,128)(2,1)} %param.25) | copy-start | bytes 294916
  6.5 101.8 %all-gather.13.cloned.1.call-start = ((), (), s32[]{:S(2)}) async-start(), calls=%async_computation.7 | async-start | bytes 2359296 | tf_op jit(solution)/shard_map/all_gather | solution.py:20
  7.6 22.7 %collective-permute-start = (bf16[3,512]{0,1:T(8,128)(2,1)S(1)}, bf16[3,512]{0,1:T(8,128)(2,1)S(1)}, u32[]{:S(2)}, u32[]{:S(2)}) collective-permute-start(bf16[3,512]{0,1:T(8,128)(2,1)S(1)} %copy.49), channel_id=1, source_target_pairs={{0,4},{4,8},{8,12},{12,16},{16,20},{20,24},{24,28},{1,5},{5,9},{9,... | collective-permute-start | bytes 9224 | tf_op jit(solution)/shard_map/ppermute | solution.py:15
  13.3 15.7 %collective-permute-start.2 = (bf16[3,64]{0,1:T(8,128)(2,1)S(1)}, bf16[3,64]{0,1:T(8,128)(2,1)S(1)}, u32[]{:S(2)}, u32[]{:S(2)}) collective-permute-start(bf16[3,64]{0,1:T(8,128)(2,1)S(1)} %slice.146), channel_id=1, source_target_pairs={{0,4},{4,8},{8,12},{12,16},{16,20},{20,24},{24,28},{1,5},{5,9},{9,... | collective-permute-start | bytes 1160 | tf_op jit(solution)/shard_map/ppermute | solution.py:15
  42.3 23.1 %copy-start.25 = (u32[32]{0:T(128)S(1)}, u32[32]{0:T(128)}, u32[]{:S(2)}) copy-start(u32[32]{0:T(128)} %constant.110) | copy-start | bytes 388
  42.3 25.2 %copy-start.20 = (bf16[4,64]{1,0:T(4,128)(2,1)S(1)}, bf16[4,64]{1,0:T(4,128)(2,1)}, u32[]{:S(2)}) copy-start(bf16[4,64]{1,0:T(4,128)(2,1)} %param.34) | copy-start | bytes 1540
  57.9 0.7 copy-start.2
  57.9 31.4 %copy-start.21 = (f32[64]{0:T(128)S(1)}, f32[64]{0:T(128)}, u32[]{:S(2)}) copy-start(f32[64]{0:T(128)} %get-tuple-element.241) | copy-start | bytes 772
  57.9 31.4 %copy-start.22 = (f32[64]{0:T(128)S(1)}, f32[64]{0:T(128)}, u32[]{:S(2)}) copy-start(f32[64]{0:T(128)} %get-tuple-element.242) | copy-start | bytes 772
  57.9 31.4 %copy-start.23 = (f32[64]{0:T(128)S(1)}, f32[64]{0:T(128)}, u32[]{:S(2)}) copy-start(f32[64]{0:T(128)} %get-tuple-element.243) | copy-start | bytes 772
  58.7 125.7 %reduce-scatter.3.cloned.1.call-start = ((), (), s32[]{:S(2)}) async-start(), calls=%async_computation.2 | async-start | bytes 7864320 | tf_op jit(solution)/shard_map/reduce_scatter | solution.py:157
  59.5 28.4 %collective-permute-start.1 = (bf16[3,64]{0,1:T(8,128)(2,1)S(1)}, bf16[3,64]{0,1:T(8,128)(2,1)S(1)}, u32[]{:S(2)}, u32[]{:S(2)}) collective-permute-start(bf16[3,64]{0,1:T(8,128)(2,1)S(1)} %slice.137), channel_id=1, source_target_pairs={{0,4},{4,8},{8,12},{12,16},{16,20},{20,24},{24,28},{1,5},{5,9},{9,... | collective-permute-start | bytes 1160 | tf_op jit(solution)/shard_map/ppermute | solution.py:15
  108.3 10.7 %copy-start.26 = (f32[6,128,128]{2,1,0:T(8,128)S(1)}, f32[6,128,128]{2,1,0:T(8,128)}, u32[]{:S(2)}) copy-start(f32[6,128,128]{2,1,0:T(8,128)} %fusion.51) | copy-start | bytes 1179652
  116.0 3.0 copy-start.15
  120.3 1.1 copy-start.3
  120.3 1.7 copy-start.24
  126.8 59.5 %copy-start.19 = (f32[2048]{0:T(1024)S(1)}, f32[2048]{0:T(1024)}, u32[]{:S(2)}) copy-start(f32[2048]{0:T(1024)} %param.38) | copy-start | bytes 24580
  126.8 60.7 %copy-start.4 = (bf16[1408,256]{1,0:T(8,128)(2,1)S(1)}, bf16[1408,256]{1,0:T(8,128)(2,1)}, u32[]{:S(2)}) copy-start(bf16[1408,256]{1,0:T(8,128)(2,1)} %param.43) | copy-start | bytes 2162692
  126.8 284.8 %all-gather.11.cloned.1.call-start = ((), (), s32[]{:S(2)}) async-start(), calls=%async_computation.5 | async-start | bytes 6488064 | tf_op jit(solution)/shard_map/all_gather | solution.py:168
  127.6 236.0 %copy-start.17 = (bf16[3,1408]{1,0:T(4,128)(2,1)S(1)}, bf16[3,1408]{1,0:T(4,128)(2,1)}, u32[]{:S(2)}) copy-start(bf16[3,1408]{1,0:T(4,128)(2,1)} %param.42) | copy-start | bytes 25348
  127.6 236.0 %copy-start.18 = (bf16[3,1408]{1,0:T(4,128)(2,1)S(1)}, bf16[3,1408]{1,0:T(4,128)(2,1)}, u32[]{:S(2)}) copy-start(bf16[3,1408]{1,0:T(4,128)(2,1)} %param.41) | copy-start | bytes 25348
  127.6 284.0 %all-gather.7.cloned.1.call-start = ((), (), s32[]{:S(2)}) async-start(), calls=%async_computation.3 | async-start | bytes 3932160 | tf_op jit(solution)/shard_map/all_gather | solution.py:165
  187.5 273.5 %all-gather.9.cloned.1.call-start = ((), (), s32[]{:S(2)}) async-start(), calls=%async_computation.4 | async-start | bytes 6488064 | tf_op jit(solution)/shard_map/all_gather | solution.py:167
  187.5 29.2 %collective-permute-start.5 = (bf16[1408,256]{1,0:T(8,128)(2,1)S(1)}, bf16[1408,256]{1,0:T(8,128)(2,1)S(1)}, u32[]{:S(2)}, u32[]{:S(2)}) collective-permute-start(bf16[1408,256]{1,0:T(8,128)(2,1)S(1)} %copy-done.4), channel_id=1, source_target_pairs={{0,4},{4,8},{8,12},{12,16},{16,20},{20,24},{24,28},{28,0},{1,5},{5... | collective-permute-start | bytes 2162696 | tf_op jit(solution)/shard_map/ppermute | solution.py:184
  189.0 339.8 %reduce-scatter.5.cloned.1.call-start = ((), (), s32[]{:S(2)}) async-start(), calls=%async_computation.6 | async-start | bytes 3932160 | tf_op jit(solution)/shard_map/reduce_scatter | solution.py:189
  216.7 30.0 %collective-permute-start.6 = (bf16[1408,256]{1,0:T(8,128)(2,1)S(1)}, bf16[1408,256]{1,0:T(8,128)(2,1)S(1)}, u32[]{:S(2)}, u32[]{:S(2)}) collective-permute-start(bf16[1408,256]{1,0:T(8,128)(2,1)S(1)} %collective-permute-done.5), channel_id=1, source_target_pairs={{0,4},{4,8},{8,12},{12,16},{16,20},{20,24},{24,28},{28,0},{1,5},{5... | collective-permute-start | bytes 2162696 | tf_op jit(solution)/shard_map/ppermute | solution.py:184
  246.7 0.9 copy-start.5
  247.6 36.3 %collective-permute-start.7 = (bf16[1408,256]{1,0:T(8,128)(2,1)S(1)}, bf16[1408,256]{1,0:T(8,128)(2,1)S(1)}, u32[]{:S(2)}, u32[]{:S(2)}) collective-permute-start(bf16[1408,256]{1,0:T(8,128)(2,1)S(1)} %collective-permute-done.6), channel_id=1, source_target_pairs={{0,4},{4,8},{8,12},{12,16},{16,20},{20,24},{24,28},{28,0},{1,5},{5... | collective-permute-start | bytes 2162696 | tf_op jit(solution)/shard_map/ppermute | solution.py:184
  283.9 0.9 copy-start.7
  284.8 36.1 %collective-permute-start.8 = (bf16[1408,256]{1,0:T(8,128)(2,1)S(1)}, bf16[1408,256]{1,0:T(8,128)(2,1)S(1)}, u32[]{:S(2)}, u32[]{:S(2)}) collective-permute-start(bf16[1408,256]{1,0:T(8,128)(2,1)S(1)} %collective-permute-done.7), channel_id=1, source_target_pairs={{0,4},{4,8},{8,12},{12,16},{16,20},{20,24},{24,28},{28,0},{1,5},{5... | collective-permute-start | bytes 2162696 | tf_op jit(solution)/shard_map/ppermute | solution.py:184
  320.9 0.9 copy-start.9
  321.8 21.2 %collective-permute-start.9 = (bf16[1408,256]{1,0:T(8,128)(2,1)S(1)}, bf16[1408,256]{1,0:T(8,128)(2,1)S(1)}, u32[]{:S(2)}, u32[]{:S(2)}) collective-permute-start(bf16[1408,256]{1,0:T(8,128)(2,1)S(1)} %collective-permute-done.8), channel_id=1, source_target_pairs={{0,4},{4,8},{8,12},{12,16},{16,20},{20,24},{24,28},{28,0},{1,5},{5... | collective-permute-start | bytes 2162696 | tf_op jit(solution)/shard_map/ppermute | solution.py:184
  343.0 0.9 copy-start.11
  343.9 19.7 %collective-permute-start.10 = (bf16[1408,256]{1,0:T(8,128)(2,1)S(1)}, bf16[1408,256]{1,0:T(8,128)(2,1)}, u32[]{:S(2)}, u32[]{:S(2)}) collective-permute-start(bf16[1408,256]{1,0:T(8,128)(2,1)S(1)} %collective-permute-done.9), channel_id=1, source_target_pairs={{0,4},{4,8},{8,12},{12,16},{16,20},{20,24},{24,28},{28,0},{1,5},{5... | collective-permute-start | bytes 2162696 | tf_op jit(solution)/shard_map/ppermute | solution.py:184
  363.6 27.9 %collective-permute-start.11 = (bf16[1408,256]{1,0:T(8,128)(2,1)}, bf16[1408,256]{1,0:T(8,128)(2,1)}, u32[]{:S(2)}, u32[]{:S(2)}) collective-permute-start(bf16[1408,256]{1,0:T(8,128)(2,1)} %collective-permute-done.10), channel_id=1, source_target_pairs={{0,4},{4,8},{8,12},{12,16},{16,20},{20,24},{24,28},{28,0},{1,5},{5... | collective-permute-start | bytes 2162696 | tf_op jit(solution)/shard_map/ppermute | solution.py:184
  363.6 32.1 %copy-start.12 = (bf16[1408,256]{1,0:T(8,128)(2,1)S(1)}, bf16[1408,256]{1,0:T(8,128)(2,1)}, u32[]{:S(2)}) copy-start(bf16[1408,256]{1,0:T(8,128)(2,1)} %copy-done.11) | copy-start | bytes 2162692
  363.6 33.1 %copy-start.10 = (bf16[1408,256]{1,0:T(8,128)(2,1)S(1)}, bf16[1408,256]{1,0:T(8,128)(2,1)}, u32[]{:S(2)}) copy-start(bf16[1408,256]{1,0:T(8,128)(2,1)} %copy-done.9) | copy-start | bytes 2162692
  363.6 34.0 %copy-start.8 = (bf16[1408,256]{1,0:T(8,128)(2,1)S(1)}, bf16[1408,256]{1,0:T(8,128)(2,1)}, u32[]{:S(2)}) copy-start(bf16[1408,256]{1,0:T(8,128)(2,1)} %copy-done.7) | copy-start | bytes 2162692
  393.5 5.1 copy-start.6
  419.9 1.4 copy-start.13
  421.4 50.7 %collective-permute-start.4 = (bf16[2,1408]{1,0:T(2,128)(2,1)S(1)}, bf16[2,1408]{1,0:T(2,128)(2,1)S(1)}, u32[]{:S(2)}, u32[]{:S(2)}) collective-permute-start(bf16[2,1408]{1,0:T(2,128)(2,1)S(1)} %slice.186), channel_id=1, source_target_pairs={{0,4},{4,8},{8,12},{12,16},{16,20},{20,24},{24,28},{1,5},{5,9},{9,... | collective-permute-start | bytes 16904 | tf_op jit(solution)/shard_map/ppermute | solution.py:15
  461.0 11.0 %copy-start.14 = (bf16[768,1408]{1,0:T(8,128)(2,1)S(1)}, bf16[768,1408]{1,0:T(8,128)(2,1)}, u32[]{:S(2)}) copy-start(bf16[768,1408]{1,0:T(8,128)(2,1)} %copy-done.13) | copy-start | bytes 6488068
  469.5 3.9 collective-permute-start.3
  475.8 55.4 %copy-start.1 = (bf16[512,2048]{1,0:T(8,128)(2,1)S(1)}, bf16[512,2048]{1,0:T(8,128)(2,1)}, u32[]{:S(2)}) copy-start(bf16[512,2048]{1,0:T(8,128)(2,1)} %param.36) | copy-start | bytes 6291460
Sparse Core Ops, SparseCore 0:
  58.8 49.4 all-gather.12
  126.9 57.4 reduce-scatter.2
  186.6 133.7 all-gather.10
  321.8 38.7 all-gather.6
  362.6 98.2 all-gather.8
  490.2 38.6 reduce-scatter.4
